TPU v7x, 32 devices: a whole 2x2x4 slice. The times are simulated.
32 devices in a mesh: ep: 8 (over z, x), tp: 4 (over y, core).
Axes of the slice: x: 2, y: 2, z: 4, core: 2. Of those that a mesh axis runs over, the one named last changes fastest.
Arguments:
- tokens: bfloat16 [1024, 4096], P('ep', 'tp'), may hold values from -16 to 16
- expert_ids: int32 [1024, 2], P('ep'), may hold values from 0 to 7, as said below
- group_weight: float32 [1024], P('ep'), may hold values from 0.25 to 1
- expert_weight: float32 [1024, 2], P('ep'), may hold values from 0.1 to 1
- w_gate: bfloat16 [8, 4096, 512], P('ep', None, 'tp'), may hold values from -0.09375 to 0.09375
- w_up: bfloat16 [8, 4096, 512], P('ep', None, 'tp'), may hold values from -0.09375 to 0.09375
- w_down: bfloat16 [8, 512, 4096], P('ep', None, 'tp'), may hold values from -0.5 to 0.5
- norm_gain: float32 [4096], P('tp'), may hold values from 0.1 to 1.9
- norm_bias: float32 [4096], P('tp'), may hold values from -3 to 3
Outputs:
- normed: bfloat16 [1024, 4096], P('ep', 'tp')
Inputs may be any that keep to these rules, and one draw needn't show every extreme that they name: `expert_ids`: each row names 2 different experts of one group, a group being 2 consecutive ids; in the rows of one ep index each group is named by a 4-th of the rows. In the rows of one ep index no expert is named more than 32 times, and in every group one expert is named exactly 32 times in the rows of every ep index.
All inputs are finite; a program needn't handle non-finite values.
Results may differ from a plain program's by a relative error of at most 0.0045.
Values may be sent and summed in bfloat16 or wider, within the bound.
A program may use at most 64 MiB of HBM per device.

v0:
```python
import jax
import jax.numpy as jnp
from jax import lax
from jax.sharding import PartitionSpec as P

D = 4096
GROUPS = 4
TOP_K = 2
residual_scale = 2.0**0.5
norm_eps = 1e-05


def on_device(
    tokens, expert_ids, group_weight, expert_weight, w_gate, w_up, w_down, norm_gain, norm_bias
):
    tok_count = tokens.shape[0]
    expert_count = lax.axis_size("ep")
    capacity = min(tok_count // GROUPS, 3 * TOP_K * tok_count // (2 * expert_count))
    pair_count = tok_count * TOP_K
    flat_ids = expert_ids.reshape(pair_count)
    one_hot = (flat_ids[:, None] == jnp.arange(expert_count, dtype=jnp.int32)[None, :]).astype(
        jnp.float32
    )
    earlier = (jnp.arange(pair_count)[:, None] > jnp.arange(pair_count)[None, :]).astype(
        jnp.float32
    )
    prior_counts = jnp.dot(
        earlier, one_hot, preferred_element_type=jnp.float32, precision=lax.Precision.HIGHEST
    )
    slot_index = jnp.sum(prior_counts * one_hot, axis=1).astype(jnp.int32)
    position = flat_ids * capacity + slot_index
    owner_token = jnp.arange(pair_count, dtype=jnp.int32) // TOP_K
    slot_table = (
        jnp.full((expert_count * capacity,), tok_count, jnp.int32).at[position].set(owner_token)
    )
    gate_local = w_gate[0]
    up_local = w_up[0]
    down_local = w_down[0]
    padded = jnp.concatenate([tokens, jnp.zeros((1, tokens.shape[1]), tokens.dtype)], axis=0)
    outgoing = padded[slot_table].reshape(expert_count, capacity, tokens.shape[1])
    arrived = lax.all_to_all(outgoing, "ep", split_axis=0, concat_axis=0, tiled=True)
    sources, slot_count, slice_width = arrived.shape
    row_block = arrived.reshape(sources * slot_count, slice_width)
    row_piece = lax.all_gather(row_block, "tp", axis=1, tiled=True)
    gate_sum = jnp.dot(row_piece, gate_local, preferred_element_type=jnp.float32)
    up_sum = jnp.dot(row_piece, up_local, preferred_element_type=jnp.float32)
    hidden = (jax.nn.silu(gate_sum) * up_sum).astype(jnp.bfloat16)
    result = jnp.dot(
        lax.all_gather(hidden, "tp", axis=1, tiled=True),
        down_local,
        preferred_element_type=jnp.float32,
    )
    result = result.astype(jnp.bfloat16).reshape(sources, slot_count, down_local.shape[1])
    returned = lax.all_to_all(result, "ep", split_axis=0, concat_axis=0, tiled=True)
    flat_rows = returned.reshape(expert_count * capacity, returned.shape[2])
    picked = flat_rows[position].reshape(tok_count, TOP_K, returned.shape[2]).astype(jnp.float32)
    share_weight = (
        group_weight[:, None] * expert_weight / jnp.sum(expert_weight, axis=1, keepdims=True)
    )
    routed = jnp.einsum("tk,tkd->td", share_weight, picked)
    mixed = residual_scale * tokens.astype(jnp.float32) + routed
    first_sum, second_sum = lax.psum((jnp.sum(mixed, axis=1), jnp.sum(mixed * mixed, axis=1)), "tp")
    center = first_sum / D
    spread = second_sum / D - center * center
    centered = mixed - center[:, None]
    normed = (
        centered * lax.rsqrt(spread + norm_eps)[:, None] * norm_gain[None, :] + norm_bias[None, :]
    )
    return normed.astype(jnp.bfloat16)


def solution(mesh):
    return jax.shard_map(
        on_device,
        mesh=mesh,
        in_specs=(
            P("ep", "tp"),
            P("ep", None),
            P("ep"),
            P("ep", None),
            P("ep", None, "tp"),
            P("ep", None, "tp"),
            P("ep", None, "tp"),
            P("tp"),
            P("tp"),
        ),
        out_specs=P("ep", "tp"),
        check_vma=False,
    )
```

profile of v0, /device:TPU:0, one launch (start us, length us, event | category | flops | bytes accessed | tf_op | source)
XLA Modules:
  0.0 102.6 jit_solution(2581811494604423040)
XLA Ops:
  6.5 0.0 copy-start
  6.5 0.0 all-gather.2.cloned.1.call-start
  6.5 0.9 copy.11
  7.4 0.7 broadcast_multiply_fusion
  8.1 0.1 eq.15
  8.2 0.2 fusion.1
  8.5 0.1 copy.10
  8.6 0.1 mul.68
  8.7 1.4 %scatter_custom_fusion = s32[256]{0:T(256)S(1)} fusion(s32[256]{0:T(256)S(1)} %bitcast.33, s32[256]{0:T(256)S(1)} %and_select_fusion, s32[]{:T(128)} %constant.31.clone.1), kind=kCustom, calls=%fused_computation.30 | custom fusion | bytes 1028 | tf_op jit(solution)/shard_map/scatter | solution.py:34
  10.1 1.0 concatenate.3
  11.1 0.0 copy-start.3
  11.1 1.2 %gather_fusion = bf16[256,1024]{1,0:T(8,128)(2,1)S(1)} fusion(bf16[129,1024]{1,0:T(8,128)(2,1)S(1)} %concatenate.3, s32[1024]{0:T(1024)S(1)} %pad_clamp_fusion.1), kind=kCustom, calls=%fused_computation | custom fusion | bytes 1049600 | tf_op jit(solution)/shard_map/gather | solution.py:40
  12.3 21.7 %all_to_all.10 = bf16[8,32,1024]{2,1,0:T(8,128)(2,1)} all-to-all(bf16[8,32,1024]{2,1,0:T(8,128)(2,1)S(1)} %bitcast.31), channel_id=1, replica_groups=mesh['ep'=8,'tp'=4] {'ep'}, dimensions={0} | all-to-all | bytes 1048576 | tf_op jit(solution)/shard_map/all_to_all | solution.py:41
  34.0 0.0 copy-start.8
  34.0 0.0 all-gather.2.cloned.1.call-update
  34.0 21.8 %all-gather.2.cloned.1.call-done = bf16[256,4096]{1,0:T(8,128)(2,1)} async-done(((bf16[256,1024]{1,0:T(8,128)(2,1)}), bf16[256,4096]{1,0:T(8,128)(2,1)}) %all-gather.2.cloned.1.call-update) | async-done | bytes 2097168 | tf_op jit(solution)/shard_map/all_gather | solution.py:44
  55.8 0.0 copy-done.3
  55.8 0.0 copy-start.2
  55.8 2.5 %fusion.4 = f32[256,128]{1,0:T(8,128)S(1)} fusion(bf16[256,4096]{1,0:T(8,128)(2,1)} %all-gather.2.cloned.1.call-done, bf16[1,4096,128]{2,1,0:T(8,128)(2,1)S(1)} %copy-done.3), kind=kOutput, calls=%fused_computation.10 | convolution fusion | flops 268435456 | bytes 3276800 | tf_op jit(solution)/shard_map/dot_general | solution.py:45
  58.3 0.0 copy-done.8
  58.3 0.0 copy-done.2
  58.3 0.7 fusion
  59.0 0.0 copy-start.6
  59.0 0.0 copy-start.7
  59.0 5.8 %all_gather.7 = bf16[256,512]{1,0:T(8,128)(2,1)S(1)} all-gather(bf16[256,128]{1,0:T(8,128)(2,1)S(1)} %fusion), channel_id=1, replica_groups=mesh['ep'=8,'tp'=4] {'tp'}, dimensions={1}, use_global_device_ids=true | all-gather | bytes 327680 | tf_op jit(solution)/shard_map/all_gather | solution.py:49
  64.8 0.0 copy-done
  64.8 1.3 %convolution_convert_fusion = bf16[256,1024]{1,0:T(8,128)(2,1)} fusion(bf16[256,512]{1,0:T(8,128)(2,1)S(1)} %all_gather.7, bf16[1,512,1024]{2,1,0:T(8,128)(2,1)S(1)} %copy-done), kind=kOutput, calls=%fused_computation.3 | convolution fusion | flops 268697600 | bytes 1835008 | tf_op jit(solution)/shard_map/dot_general | solution.py:48
  66.1 5.5 %all-to-all-start.1 = ((bf16[8,32,1024]{2,1,0:T(8,128)(2,1)}), bf16[8,32,1024]{2,1,0:T(8,128)(2,1)S(1)}, u32[]{:S(2)}, u32[]{:S(2)}) async-start(bf16[8,32,1024]{2,1,0:T(8,128)(2,1)} %bitcast.8), calls=%async_computation.1 | async-start | bytes 1048576 | tf_op jit(solution)/shard_map/all_to_all | solution.py:54
  71.6 0.0 copy-done.6
  71.6 0.0 copy-done.7
  71.7 0.1 copy.12
  71.8 14.8 %all-to-all-done.1 = bf16[8,32,1024]{2,1,0:T(8,128)(2,1)S(1)} async-done(((bf16[8,32,1024]{2,1,0:T(8,128)(2,1)}), bf16[8,32,1024]{2,1,0:T(8,128)(2,1)S(1)}, u32[]{:S(2)}, u32[]{:S(2)}) %all-to-all-start.1) | async-done | bytes 524320 | tf_op jit(solution)/shard_map/all_to_all | solution.py:54
  86.6 1.2 %gather_fusion.1 = bf16[256,1024]{1,0:T(8,128)(2,1)S(1)} fusion(bf16[256,1024]{1,0:T(8,128)(2,1)S(1)} %bitcast.30, s32[1024]{0:T(1024)S(1)} %pad_clamp_fusion), kind=kCustom, calls=%fused_computation.1 | custom fusion | bytes 1049600 | tf_op jit(solution)/shard_map/gather | solution.py:56
  87.8 0.0 copy-start.1
  87.8 0.0 copy-start.4
  87.8 0.0 copy-start.5
  87.8 0.2 reshape.59
  88.0 0.7 fusion.10
  88.7 0.0 copy-done.1
  88.7 0.2 fusion.6
  88.9 5.9 %all-reduce.1 = (f32[128]{0:T(128)S(1)}, f32[128]{0:T(128)S(1)}) all-reduce(f32[128]{0:T(128)S(1)} %get-tuple-element.6, f32[128]{0:T(128)S(1)} %get-tuple-element.5), channel_id=1, replica_groups=mesh['ep'=8,'tp'=4] {'tp'}, use_global_device_ids=true, to_apply=%region_6.7 | all-reduce | flops 256 | bytes 2048 | tf_op jit(solution)/shard_map/psum | solution.py:62
  94.9 0.0 copy-done.4
  94.9 0.0 copy-done.5
  94.9 0.9 add_convert_fusion
  (9 shorter events, 0.1 us)
Async XLA Ops:
  6.5 58.3 %copy-start = (bf16[1,512,1024]{2,1,0:T(8,128)(2,1)S(1)}, bf16[1,512,1024]{2,1,0:T(8,128)(2,1)}, u32[]{:S(2)}) copy-start(bf16[1,512,1024]{2,1,0:T(8,128)(2,1)} %param.15) | copy-start | bytes 3145732
  6.5 49.3 %all-gather.2.cloned.1.call-start = ((), (), s32[]{:S(2)}) async-start(), calls=%async_computation.2 | async-start | bytes 2621440 | tf_op jit(solution)/shard_map/all_gather | solution.py:44
  11.1 44.7 %copy-start.3 = (bf16[1,4096,128]{2,1,0:T(8,128)(2,1)S(1)}, bf16[1,4096,128]{2,1,0:T(8,128)(2,1)}, u32[]{:S(2)}) copy-start(bf16[1,4096,128]{2,1,0:T(8,128)(2,1)} %param.13) | copy-start | bytes 3145732
  34.0 24.2 %copy-start.8 = (bf16[1,4096,128]{2,1,0:T(8,128)(2,1)S(1)}, bf16[1,4096,128]{2,1,0:T(8,128)(2,1)}, u32[]{:S(2)}) copy-start(bf16[1,4096,128]{2,1,0:T(8,128)(2,1)} %param.14) | copy-start | bytes 3145732
  55.8 2.5 %copy-start.2 = (bf16[256,4096]{1,0:T(8,128)(2,1)S(1)}, bf16[256,4096]{1,0:T(8,128)(2,1)}, u32[]{:S(2)}) copy-start(bf16[256,4096]{1,0:T(8,128)(2,1)} %all-gather.2.cloned.1.call-done) | copy-start | bytes 6291460
  59.0 12.6 %copy-start.6 = (f32[128,2]{0,1:T(2,128)S(1)}, f32[128,2]{0,1:T(2,128)}, u32[]{:S(2)}) copy-start(f32[128,2]{0,1:T(2,128)} %param.12) | copy-start | bytes 3076
  59.0 12.6 %copy-start.7 = (f32[128]{0:T(128)S(1)}, f32[128]{0:T(128)}, u32[]{:S(2)}) copy-start(f32[128]{0:T(128)} %param.11) | copy-start | bytes 1540
  66.1 20.5 %all-to-all-start.1 = ((bf16[8,32,1024]{2,1,0:T(8,128)(2,1)}), bf16[8,32,1024]{2,1,0:T(8,128)(2,1)S(1)}, u32[]{:S(2)}, u32[]{:S(2)}) async-start(bf16[8,32,1024]{2,1,0:T(8,128)(2,1)} %bitcast.8), calls=%async_computation.1 | async-start | bytes 1048576 | tf_op jit(solution)/shard_map/all_to_all | solution.py:54
  87.8 1.0 copy-start.1
  87.8 7.1 %copy-start.4 = (f32[1024]{0:T(1024)S(1)}, f32[1024]{0:T(1024)}, u32[]{:S(2)}) copy-start(f32[1024]{0:T(1024)} %param.17) | copy-start | bytes 12292
  87.8 7.1 %copy-start.5 = (f32[1024]{0:T(1024)S(1)}, f32[1024]{0:T(1024)}, u32[]{:S(2)}) copy-start(f32[1024]{0:T(1024)} %param.16) | copy-start | bytes 12292
Sparse Core Ops, SparseCore 0:
  34.2 21.5 all-gather.1
where the time goes:
time: 103 us
  waiting for transfers between devices  36.6 us (36%)
  blocking collectives  33.5 us (33%)
  between operations  13.6 us (13%)
  local copies, waits for them, and re-layouts  6.37 us (6%)
  starting transfers between devices  5.51 us (5%)
  matrix products  5.3 us (5%)
  other arithmetic  1.85 us (2%)
    all_gather x1, waiting for transfers between devices, on_device(): row_piece = lax.all_gather(row_block, 'tp', axis=1, tiled=True)  21.8 us
    all_to_all x1, blocking collectives, on_device(): lax.all_to_all(outgoing, 'ep', split_axis=0, concat_axis=0, tiled=True)  21.7 us
    all_to_all x1, waiting for transfers between devices, on_device(): lax.all_to_all(result, 'ep', split_axis=0, concat_axis=0, tiled=True)  14.8 us
    psum x1, blocking collectives, on_device(): lax.psum((jnp.sum(mixed, axis=1), jnp.sum(mixed * mixed, axis=1)), 'tp')  5.93 us
    all_gather x1, blocking collectives, on_device(): lax.all_gather(hidden, 'tp', axis=1, tiled=True)  5.81 us
    all_to_all x1, starting transfers between devices, on_device(): lax.all_to_all(result, 'ep', split_axis=0, concat_axis=0, tiled=True)  5.51 us
    dot_general x1, matrix products, on_device(): jnp.dot(row_piece, gate_local, preferred_element_type=jnp.float32)  2.45 us
  transfers between devices with their start and end apart: 2, of which 2 were waited for; matrix products, arithmetic and copies ran while one was open for 0% of the time, Pallas kernels for 0%

commit v1 on v0

--- a/solution.py
+++ b/solution.py
@@ -41,7 +41,12 @@
     arrived = lax.all_to_all(outgoing, "ep", split_axis=0, concat_axis=0, tiled=True)
     sources, slot_count, slice_width = arrived.shape
     row_block = arrived.reshape(sources * slot_count, slice_width)
-    row_piece = lax.all_gather(row_block, "tp", axis=1, tiled=True)
+    ring = [row_block]
+    for hop in range(3):
+        ring.append(lax.ppermute(ring[-1], "tp", [(dev, (dev + 1) % 4) for dev in range(4)]))
+    row_piece = jnp.roll(
+        jnp.concatenate(ring[::-1], axis=1), (lax.axis_index("tp") + 1) * ring[0].shape[1], axis=1
+    )
     gate_sum = jnp.dot(row_piece, gate_local, preferred_element_type=jnp.float32)
     up_sum = jnp.dot(row_piece, up_local, preferred_element_type=jnp.float32)
     hidden = (jax.nn.silu(gate_sum) * up_sum).astype(jnp.bfloat16)

time: 103 us -> 90.3 us (0.88)
  between operations: 13.6 us -> 0.22 us
  waiting for transfers between devices: 36.6 us -> 40.7 us
  starting transfers between devices: 5.51 us -> 3.6 us
  matrix products: 5.3 us -> 3.51 us
    ppermute x0 -> x3, waiting for transfers between devices: none -> 25.8 us  [on_device(): lax.ppermute(ring[-1], 'tp', [(dev, (dev + 1) % 4) for dev in range(4)])]
    all_gather x1 -> x0, waiting for transfers between devices: 21.8 us -> none  [on_device(): row_piece = lax.all_gather(row_block, 'tp', axis=1, tiled=True)]
    all_to_all x1, starting transfers between devices: 5.51 us -> 3.6 us  [on_device(): lax.all_to_all(result, 'ep', split_axis=0, concat_axis=0, tiled=True)]
    dot_general x1, matrix products: 2.45 us -> 0.7 us  [on_device(): jnp.dot(row_piece, gate_local, preferred_element_type=jnp.float32)]
  transfers between devices with their start and end apart: 2 -> 4, of which waited for: 2 -> 4; matrix products, arithmetic and copies ran while one was open for 0% -> 0% of each run, Pallas kernels for 0% -> 0%
where the time goes in v1:
time: 90.3 us; the launch traced here: 90 us
  waiting for transfers between devices  40.7 us (45%)
  blocking collectives  33.2 us (37%)
  local copies, waits for them, and re-layouts  6.9 us (8%)
  starting transfers between devices  3.6 us (4%)
  matrix products  3.51 us (4%)
  other arithmetic  1.85 us (2%)
    ppermute x3, waiting for transfers between devices, on_device(): lax.ppermute(ring[-1], 'tp', [(dev, (dev + 1) % 4) for dev in range(4)])  25.8 us
    all_to_all x1, blocking collectives, on_device(): lax.all_to_all(outgoing, 'ep', split_axis=0, concat_axis=0, tiled=True)  21.6 us
    all_to_all x1, waiting for transfers between devices, on_device(): lax.all_to_all(result, 'ep', split_axis=0, concat_axis=0, tiled=True)  14.9 us
    all_gather x1, blocking collectives, on_device(): lax.all_gather(hidden, 'tp', axis=1, tiled=True)  5.83 us
    psum x1, blocking collectives, on_device(): lax.psum((jnp.sum(mixed, axis=1), jnp.sum(mixed * mixed, axis=1)), 'tp')  5.77 us
    all_to_all x1, starting transfers between devices, on_device(): lax.all_to_all(result, 'ep', split_axis=0, concat_axis=0, tiled=True)  3.6 us
  transfers between devices with their start and end apart: 4, of which 4 were waited for; matrix products, arithmetic and copies ran while one was open for 0% of the time, Pallas kernels for 0%

profile of v1, /device:TPU:0, one launch (start us, length us, event | category | flops | bytes accessed | tf_op | source)
XLA Modules:
  0.0 90.0 jit_solution(2677183154476733930)
XLA Ops:
  0.0 0.0 copy-start
  0.0 0.9 copy.11
  0.9 0.7 broadcast_multiply_fusion
  1.6 0.1 eq.18
  1.7 0.2 fusion.4
  1.9 0.1 copy.10
  2.0 0.1 mul.71
  2.2 1.4 %scatter_custom_fusion = s32[256]{0:T(256)S(1)} fusion(s32[256]{0:T(256)S(1)} %bitcast.35, s32[256]{0:T(256)S(1)} %and_select_fusion, s32[]{:T(128)} %constant.54.clone.1), kind=kCustom, calls=%fused_computation.40 | custom fusion | bytes 1028 | tf_op jit(solution)/shard_map/scatter | solution.py:34
  3.6 1.0 %concatenate.9 = bf16[129,1024]{1,0:T(8,128)(2,1)S(1)} pad(bf16[128,1024]{1,0:T(8,128)(2,1)} %param.9, bf16[]{:T(256)} %constant.53.clone.1), padding=0_1x0_0 | pad | bytes 526338 | tf_op jit(solution)/shard_map/concatenate | solution.py:39
  4.6 1.2 %gather_fusion = bf16[256,1024]{1,0:T(8,128)(2,1)S(1)} fusion(bf16[129,1024]{1,0:T(8,128)(2,1)S(1)} %concatenate.9, s32[1024]{0:T(1024)S(1)} %pad_clamp_fusion.1), kind=kCustom, calls=%fused_computation | custom fusion | bytes 1049600 | tf_op jit(solution)/shard_map/gather | solution.py:40
  5.8 21.6 %all_to_all.10 = bf16[8,32,1024]{2,1,0:T(8,128)(2,1)S(1)} all-to-all(bf16[8,32,1024]{2,1,0:T(8,128)(2,1)S(1)} %bitcast.34), channel_id=1, replica_groups=mesh['ep'=8,'tp'=4] {'ep'}, dimensions={0} | all-to-all | bytes 1048576 | tf_op jit(solution)/shard_map/all_to_all | solution.py:41
  27.4 0.0 collective-permute-start
  27.4 8.6 %collective-permute-done = bf16[256,1024]{1,0:T(8,128)(2,1)S(1)} collective-permute-done((bf16[256,1024]{1,0:T(8,128)(2,1)S(1)}, bf16[256,1024]{1,0:T(8,128)(2,1)S(1)}, u32[]{:S(2)}, u32[]{:S(2)}) %collective-permute-start) | collective-permute-done | bytes 524320 | tf_op jit(solution)/shard_map/ppermute | solution.py:46
  36.0 0.0 collective-permute-start.1
  36.0 8.6 %collective-permute-done.1 = bf16[256,1024]{1,0:T(8,128)(2,1)S(1)} collective-permute-done((bf16[256,1024]{1,0:T(8,128)(2,1)S(1)}, bf16[256,1024]{1,0:T(8,128)(2,1)S(1)}, u32[]{:S(2)}, u32[]{:S(2)}) %collective-permute-start.1) | collective-permute-done | bytes 524320 | tf_op jit(solution)/shard_map/ppermute | solution.py:46
  44.6 0.0 collective-permute-start.2
  44.6 0.0 copy-start.2
  44.6 8.6 %collective-permute-done.2 = bf16[256,1024]{1,0:T(8,128)(2,1)S(1)} collective-permute-done((bf16[256,1024]{1,0:T(8,128)(2,1)S(1)}, bf16[256,1024]{1,0:T(8,128)(2,1)S(1)}, u32[]{:S(2)}, u32[]{:S(2)}) %collective-permute-start.2) | collective-permute-done | bytes 524320 | tf_op jit(solution)/shard_map/ppermute | solution.py:46
  53.3 0.0 copy-start.7
  53.6 0.0 copy-done.2
  53.6 0.7 fusion.2
  54.3 0.3 copy-done.7
  54.5 0.0 copy-start.5
  54.6 0.0 copy-start.6
  54.6 0.7 multiply_convert_fusion
  55.3 5.8 %all_gather.3 = bf16[256,512]{1,0:T(8,128)(2,1)S(1)} all-gather(bf16[256,128]{1,0:T(8,128)(2,1)S(1)} %multiply_convert_fusion), channel_id=1, replica_groups=mesh['ep'=8,'tp'=4] {'tp'}, dimensions={1}, use_global_device_ids=true | all-gather | bytes 327680 | tf_op jit(solution)/shard_map/all_gather | solution.py:54
  61.1 0.0 copy-done
  61.1 1.2 %convolution_convert_fusion = bf16[256,1024]{1,0:T(8,128)(2,1)} fusion(bf16[256,512]{1,0:T(8,128)(2,1)S(1)} %all_gather.3, bf16[1,512,1024]{2,1,0:T(8,128)(2,1)S(1)} %copy-done), kind=kOutput, calls=%fused_computation.7 | convolution fusion | flops 268697600 | bytes 1835008 | tf_op jit(solution)/shard_map/dot_general | solution.py:53
  62.3 3.6 %all-to-all-start.1 = ((bf16[8,32,1024]{2,1,0:T(8,128)(2,1)}), bf16[8,32,1024]{2,1,0:T(8,128)(2,1)S(1)}, u32[]{:S(2)}, u32[]{:S(2)}) async-start(bf16[8,32,1024]{2,1,0:T(8,128)(2,1)} %bitcast.8), calls=%async_computation.1 | async-start | bytes 1048576 | tf_op jit(solution)/shard_map/all_to_all | solution.py:59
  65.9 0.0 copy-done.5
  65.9 0.0 copy-start.1
  66.0 0.0 copy-done.6
  66.0 0.1 copy.12
  66.1 14.9 %all-to-all-done.1 = bf16[8,32,1024]{2,1,0:T(8,128)(2,1)S(1)} async-done(((bf16[8,32,1024]{2,1,0:T(8,128)(2,1)}), bf16[8,32,1024]{2,1,0:T(8,128)(2,1)S(1)}, u32[]{:S(2)}, u32[]{:S(2)}) %all-to-all-start.1) | async-done | bytes 524320 | tf_op jit(solution)/shard_map/all_to_all | solution.py:59
  81.0 0.0 copy-start.3
  81.0 0.0 copy-start.4
  81.0 1.2 %gather_fusion.1 = bf16[256,1024]{1,0:T(8,128)(2,1)S(1)} fusion(bf16[256,1024]{1,0:T(8,128)(2,1)S(1)} %bitcast.30, s32[1024]{0:T(1024)S(1)} %pad_clamp_fusion), kind=kCustom, calls=%fused_computation.1 | custom fusion | bytes 1049600 | tf_op jit(solution)/shard_map/gather | solution.py:61
  82.2 0.2 reshape.59
  82.4 0.7 fusion.18
  83.1 0.0 copy-done.1
  83.1 0.2 fusion.8
  83.3 5.8 %all-reduce.1 = (f32[128]{0:T(128)S(1)}, f32[128]{0:T(128)S(1)}) all-reduce(f32[128]{0:T(128)S(1)} %get-tuple-element.6, f32[128]{0:T(128)S(1)} %get-tuple-element.5), channel_id=1, replica_groups=mesh['ep'=8,'tp'=4] {'tp'}, use_global_device_ids=true, to_apply=%region_6.7 | all-reduce | flops 256 | bytes 2048 | tf_op jit(solution)/shard_map/psum | solution.py:67
  89.1 0.0 copy-done.3
  89.1 0.0 copy-done.4
  89.1 0.9 %add_convert_fusion = bf16[128,1024]{1,0:T(8,128)(2,1)} fusion(f32[1024]{0:T(1024)S(1)} %copy-done.3, f32[1024]{0:T(1024)S(1)} %copy-done.4, f32[128]{0:T(128)S(1)} %get-tuple-element.10, f32[128]{0:T(128)S(1)} %get-tuple-element.9, f32[128,1,1024]{2,1,0:T(1,128)S(1)} %fusion.18, bf16[128,1024]{1,0:T(8,128)(2,1)S(1)} %copy-done.1), kind=kLoop, calls=%fused_computation.14 | loop fusion | flops 1048576 | bytes 1057792 | tf_op jit(solution)/shard_map/convert_element_type | solution.py:74
  (17 shorter events, 0.4 us)
Async XLA Ops:
  0.0 61.1 %copy-start = (bf16[1,512,1024]{2,1,0:T(8,128)(2,1)S(1)}, bf16[1,512,1024]{2,1,0:T(8,128)(2,1)}, u32[]{:S(2)}) copy-start(bf16[1,512,1024]{2,1,0:T(8,128)(2,1)} %param.15) | copy-start | bytes 3145732
  27.4 8.6 %collective-permute-start = (bf16[256,1024]{1,0:T(8,128)(2,1)S(1)}, bf16[256,1024]{1,0:T(8,128)(2,1)S(1)}, u32[]{:S(2)}, u32[]{:S(2)}) collective-permute-start(bf16[256,1024]{1,0:T(8,128)(2,1)S(1)} %bitcast.31), channel_id=1, source_target_pairs={{0,1},{1,2},{2,3},{3,0},{4,5},{5,6},{6,7},{7,4},{8,9},{9,10},{10,1... | collective-permute-start | bytes 1572872 | tf_op jit(solution)/shard_map/ppermute | solution.py:46
  36.0 8.6 %collective-permute-start.1 = (bf16[256,1024]{1,0:T(8,128)(2,1)S(1)}, bf16[256,1024]{1,0:T(8,128)(2,1)S(1)}, u32[]{:S(2)}, u32[]{:S(2)}) collective-permute-start(bf16[256,1024]{1,0:T(8,128)(2,1)S(1)} %collective-permute-done), channel_id=1, source_target_pairs={{0,1},{1,2},{2,3},{3,0},{4,5},{5,6},{6,7},{7,4},{8,9},{9,10},{10,1... | collective-permute-start | bytes 1572872 | tf_op jit(solution)/shard_map/ppermute | solution.py:46
  44.6 8.6 %collective-permute-start.2 = (bf16[256,1024]{1,0:T(8,128)(2,1)S(1)}, bf16[256,1024]{1,0:T(8,128)(2,1)S(1)}, u32[]{:S(2)}, u32[]{:S(2)}) collective-permute-start(bf16[256,1024]{1,0:T(8,128)(2,1)S(1)} %collective-permute-done.1), channel_id=1, source_target_pairs={{0,1},{1,2},{2,3},{3,0},{4,5},{5,6},{6,7},{7,4},{8,9},{9,10},{10,1... | collective-permute-start | bytes 1572872 | tf_op jit(solution)/shard_map/ppermute | solution.py:46
  44.6 9.0 %copy-start.2 = (bf16[1,4096,128]{2,1,0:T(8,128)(2,1)S(1)}, bf16[1,4096,128]{2,1,0:T(8,128)(2,1)}, u32[]{:S(2)}) copy-start(bf16[1,4096,128]{2,1,0:T(8,128)(2,1)} %param.13) | copy-start | bytes 3145732
  53.3 1.2 %copy-start.7 = (bf16[1,4096,128]{2,1,0:T(8,128)(2,1)S(1)}, bf16[1,4096,128]{2,1,0:T(8,128)(2,1)}, u32[]{:S(2)}) copy-start(bf16[1,4096,128]{2,1,0:T(8,128)(2,1)} %param.14) | copy-start | bytes 3145732
  54.5 11.4 %copy-start.5 = (f32[128,2]{0,1:T(2,128)S(1)}, f32[128,2]{0,1:T(2,128)}, u32[]{:S(2)}) copy-start(f32[128,2]{0,1:T(2,128)} %param.12) | copy-start | bytes 3076
  54.6 11.4 %copy-start.6 = (f32[128]{0:T(128)S(1)}, f32[128]{0:T(128)}, u32[]{:S(2)}) copy-start(f32[128]{0:T(128)} %param.11) | copy-start | bytes 1540
  62.3 18.7 %all-to-all-start.1 = ((bf16[8,32,1024]{2,1,0:T(8,128)(2,1)}), bf16[8,32,1024]{2,1,0:T(8,128)(2,1)S(1)}, u32[]{:S(2)}, u32[]{:S(2)}) async-start(bf16[8,32,1024]{2,1,0:T(8,128)(2,1)} %bitcast.8), calls=%async_computation.1 | async-start | bytes 1048576 | tf_op jit(solution)/shard_map/all_to_all | solution.py:59
  65.9 17.2 %copy-start.1 = (bf16[128,1024]{1,0:T(8,128)(2,1)S(1)}, bf16[128,1024]{1,0:T(8,128)(2,1)}, u32[]{:S(2)}) copy-start(bf16[128,1024]{1,0:T(8,128)(2,1)} %param.9) | copy-start | bytes 786436
  81.0 8.1 %copy-start.3 = (f32[1024]{0:T(1024)S(1)}, f32[1024]{0:T(1024)}, u32[]{:S(2)}) copy-start(f32[1024]{0:T(1024)} %param.17) | copy-start | bytes 12292
  81.0 8.1 %copy-start.4 = (f32[1024]{0:T(1024)S(1)}, f32[1024]{0:T(1024)}, u32[]{:S(2)}) copy-start(f32[1024]{0:T(1024)} %param.16) | copy-start | bytes 12292
